TPU v7x, 32 devices: a whole 2x2x4 slice. The times are simulated.
32 devices in a mesh: sp: 16 (over z, y, x), tp: 2 (over core).
Axes of the slice: x: 2, y: 2, z: 4, core: 2. Of those that a mesh axis runs over, the one named last changes fastest.
Arguments:
- tokens_in: bfloat16 [2048, 2048], P(('sp', 'tp')), may hold values from -9 to 9, as said below
- w_query: bfloat16 [2048, 2048], P(None, 'tp'), may hold values from -0.125 to 0.125
- w_key: bfloat16 [2048, 512], P(None, 'tp'), may hold values from -0.125 to 0.125
- w_value: bfloat16 [2048, 512], P(None, 'tp'), may hold values from -0.125 to 0.125
- w_out: bfloat16 [2048, 2048], P('tp'), may hold values from -0.125 to 0.125
- q_gain: float32 [64], replicated, may hold values from 0.1 to 14
- k_gain: float32 [64], replicated, may hold values from 0.1 to 14
Outputs:
- attended: bfloat16 [2048, 2048], P(('sp', 'tp'))
Inputs may be any that keep to these rules, and one draw needn't show every extreme that they name: `tokens_in`: activations whose mean differs from one block of 128 tokens to another.
All inputs are finite; a program needn't handle non-finite values.
Results may differ from a plain program's by a relative error of at most 0.014.
The roundings to bfloat16 on the way count: a program that leaves them out, or rounds other values in their place, can miss the bound.
Values may be sent and summed in bfloat16 or wider, within the bound.
A program may use at most 64 MiB of HBM per device.

v0:
```python
import jax
import jax.numpy as jnp
from jax import lax
from jax.sharding import PartitionSpec as P

GRID_W = 64


def turned(vectors, position, gain):
    pairs = vectors.shape[-1] // 4
    scaled = vectors * lax.rsqrt(jnp.mean(vectors * vectors, axis=-1, keepdims=True) + 1e-06) * gain
    freq = 10000.0 ** (-jnp.arange(pairs, dtype=jnp.float32) / pairs)
    grid_row = (position // GRID_W).astype(jnp.float32)
    grid_col = (position % GRID_W).astype(jnp.float32)
    angle = jnp.stack([grid_row[:, None] * freq, grid_col[:, None] * freq], axis=1)
    cosine = jnp.cos(angle)[:, None]
    sine = jnp.sin(angle)[:, None]
    split = scaled.reshape(scaled.shape[:-1] + (2, 2, pairs))
    first = split[..., 0, :]
    second = split[..., 1, :]
    joined = jnp.stack([first * cosine - second * sine, first * sine + second * cosine], axis=-2)
    return joined.reshape(scaled.shape)


def body(tokens_in, w_query, w_key, w_value, w_out, q_gain, k_gain):
    head_dim = q_gain.shape[0]
    query_cols = w_query.shape[1]
    key_cols = w_key.shape[1]
    kv_heads = key_cols // head_dim
    group = query_cols // key_cols
    w_joined = jnp.concatenate([w_query, w_key, w_value], axis=1)
    projected = jnp.dot(
        lax.all_gather(tokens_in, "tp", axis=0, tiled=True),
        w_joined,
        preferred_element_type=jnp.float32,
    ).astype(jnp.bfloat16)
    row_count = projected.shape[0]
    position = lax.axis_index("sp") * row_count + jnp.arange(row_count, dtype=jnp.int32)
    query_n = turned(
        projected[:, :query_cols]
        .astype(jnp.float32)
        .reshape(row_count, kv_heads * group, head_dim),
        position,
        q_gain,
    ).astype(jnp.bfloat16)
    query_g = query_n.reshape(row_count, kv_heads, group, head_dim).transpose(1, 2, 0, 3)
    raw_keys = projected[:, query_cols : query_cols + key_cols]
    values = projected[:, query_cols + key_cols :]
    scale = head_dim ** (-0.5)
    outgoing = jnp.concatenate([raw_keys, values], axis=1)
    piece = lax.all_gather(outgoing, "sp", axis=0, tiled=True)
    length = piece.shape[0]
    spot = jnp.arange(length, dtype=jnp.int32)
    keys_n = turned(
        piece[:, :key_cols].astype(jnp.float32).reshape(length, kv_heads, head_dim), spot, k_gain
    ).astype(jnp.bfloat16)
    peak = jnp.full((kv_heads, group, row_count), -1e30, jnp.float32)
    scores = (
        jnp.einsum("kgqd,nkd->kgqn", query_g, keys_n, preferred_element_type=jnp.float32) * scale
    )
    new_peak = jnp.maximum(peak, jnp.max(scores, axis=-1))
    expo = jnp.exp(scores - new_peak[..., None])
    total = jnp.sum(expo, axis=-1)
    summed = jnp.einsum(
        "kgqn,nkd->kgqd",
        expo.astype(jnp.bfloat16),
        piece[:, key_cols:].reshape(length, kv_heads, head_dim),
        preferred_element_type=jnp.float32,
    )
    peak, total, summed = (new_peak, total, summed)
    mixed = (summed / total[..., None]).astype(jnp.bfloat16)
    mixed = mixed.transpose(2, 0, 1, 3).reshape(row_count, query_cols)
    return lax.psum_scatter(
        jnp.dot(mixed, w_out, preferred_element_type=jnp.float32).astype(jnp.bfloat16),
        "tp",
        scatter_dimension=0,
        tiled=True,
    )


def solution(mesh):
    return jax.shard_map(
        body,
        mesh=mesh,
        in_specs=(
            P(("sp", "tp"), None),
            P(None, "tp"),
            P(None, "tp"),
            P(None, "tp"),
            P("tp", None),
            P(),
            P(),
        ),
        out_specs=P(("sp", "tp"), None),
        check_vma=False,
    )
```

profile of v0, /device:TPU:0, one launch (start us, length us, event | category | flops | bytes accessed | tf_op | source)
XLA Modules:
  0.0 117.6 jit_solution(13708748384121845471)
XLA Ops:
  6.5 0.0 all-gather.2.cloned.1.call-start
  6.5 2.5 %all_gather.6 = bf16[128,2048]{1,0:T(8,128)(2,1)S(1)} all-gather(bf16[64,2048]{1,0:T(8,128)(2,1)} %param.7), channel_id=1, replica_groups=mesh['sp'=16,'tp'=2] {'tp'}, dimensions={0}, use_global_device_ids=true | all-gather | bytes 786432 | tf_op jit(solution)/shard_map/all_gather | solution.py:33
  9.0 0.0 copy-start.1
  9.0 0.0 copy-start.2
  9.0 4.1 %fusion.13 = bf16[128,1536]{0,1:T(8,128)(2,1)S(1)} fusion(bf16[128,2048]{1,0:T(8,128)(2,1)S(1)} %all_gather.6, bf16[2048,256]{1,0:T(8,128)(2,1)} %param.10, bf16[2048,256]{1,0:T(8,128)(2,1)} %param.9, bf16[2048,1024]{1,0:T(8,128)(2,1)} %param.8), kind=kOutput, calls=%fused_computation.13 | convolution fusion | flops 824377344 | bytes 7208960 | tf_op jit(solution)/shard_map/dot_general | solution.py:32
  13.1 0.7 concatenate.24
  13.8 0.0 all-gather.2.cloned.1.call-update
  13.8 0.0 reduce-scatter.2.cloned.1.call-start
  13.8 0.0 copy-done.1
  13.9 0.1 mul.221
  13.9 0.0 copy-done.2
  13.9 0.1 mul.240
  14.1 0.1 broadcast_multiply_fusion.3
  14.1 0.1 fusion.34
  14.2 0.1 bitcast_reduce_fusion.1
  14.4 0.1 multiply_multiply_fusion.1
  14.5 0.1 subtract_convert_fusion.1
  14.6 0.1 broadcast_multiply_fusion.1
  14.7 1.0 fusion.27
  15.7 63.8 %all-gather.2.cloned.1.call-done = bf16[2048,512]{0,1:T(8,128)(2,1)} async-done(((bf16[128,512]{0,1:T(8,128)(2,1)}), bf16[2048,512]{0,1:T(8,128)(2,1)}) %all-gather.2.cloned.1.call-update) | async-done | bytes 2097168 | tf_op jit(solution)/shard_map/all_gather | solution.py:51
  79.5 1.5 %bitcast_reduce_fusion = f32[2048,4]{0,1:T(4,128)S(1)} fusion(bf16[2048,512]{0,1:T(8,128)(2,1)} %all-gather.2.cloned.1.call-done), kind=kLoop, calls=%fused_computation.14 | loop fusion | flops 1564672 | bytes 1081344 | tf_op jit(solution)/shard_map/reduce_sum | solution.py:11
  81.0 1.8 %slice_convert_fusion = (f32[2048,256]{0,1:T(8,128)S(1)}, bf16[2048,256]{0,1:T(8,128)(2,1)S(1)}) fusion(bf16[2048,512]{0,1:T(8,128)(2,1)} %all-gather.2.cloned.1.call-done), kind=kLoop, calls=%fused_computation.17 | loop fusion | flops 524288 | bytes 5242880 | tf_op jit(solution)/shard_map/convert_element_type | solution.py:55
  82.9 0.4 multiply_multiply_fusion
  83.3 0.3 subtract_convert_fusion
  83.6 0.1 pad_maximum_fusion
  83.7 2.5 %multiply_reduce_fusion = (f32[4,4,128]{2,1,0:T(4,128)S(1)}, f32[4,4,128,2048]{3,2,1,0:T(8,128)S(1)}) fusion(bf16[4,4,128,64]{2,3,1,0:T(8,128)(2,1)S(1)} %bitcast.38, bf16[2048,4,64,1]{0,2,3,1:T(8,128)(2,1)S(1)} %bitcast.36), kind=kOutput, calls=%fused_computation.1 | convolution fusion | flops 545257472 | bytes 18096128 | tf_op jit(solution)/shard_map/kgqd,nkd->kgqn/dot_general | solution.py:59
  86.2 0.0 copy-start
  86.2 3.3 %fusion = f32[4,4,128]{2,1,0:T(4,128)S(1)} fusion(f32[4,4,128,2048]{3,2,1,0:T(8,128)S(1)} %get-tuple-element.20, f32[4,4,128]{2,1,0:T(4,128)S(1)} %broadcast_maximum_fusion), kind=kLoop, calls=%fused_computation.2 | loop fusion | flops 12580864 | bytes 16793600 | tf_op jit(solution)/shard_map/reduce_sum | solution.py:63
  89.5 2.4 %copy-done = f32[4,4,128,2048]{3,2,1,0:T(8,128)} copy-done((f32[4,4,128,2048]{3,2,1,0:T(8,128)}, f32[4,4,128,2048]{3,2,1,0:T(8,128)S(1)}, u32[]{:S(2)}) %copy-start) | copy-done | bytes 16777240
  91.9 8.8 %fusion.22 = bf16[128,4,4,64]{0,3,2,1:T(8,128)(2,1)S(1)} fusion(bf16[2048,4,64,1]{0,2,3,1:T(8,128)(2,1)S(1)} %bitcast.39, f32[4,4,128,2048]{3,2,1,0:T(8,128)} %copy-done, f32[4,4,128]{2,1,0:T(4,128)S(1)} %broadcast_maximum_fusion, f32[128,4,4]{0,2,1:T(4,128)S(1)} %bitcast.41), kind=kOutput, calls=%fused_computation.22 | convolution fusion | flops 549715968 | bytes 18104320 | tf_op jit(solution)/shard_map/kgqn,nkd->kgqd/dot_general | solution.py:64
  100.8 3.7 %convolution_convert_fusion = bf16[128,2048]{1,0:T(8,128)(2,1)} fusion(bf16[128,1024]{0,1:T(8,128)(2,1)S(1)} %bitcast.40, bf16[1024,2048]{1,0:T(8,128)(2,1)} %param.11), kind=kOutput, calls=%fused_computation.12 | convolution fusion | flops 537133056 | bytes 4980736 | tf_op jit(solution)/shard_map/dot_general | solution.py:74
  104.5 0.0 reduce-scatter.2.cloned.1.call-update
  104.5 6.3 %reduce-scatter.2.cloned.1.call-done = bf16[64,2048]{1,0:T(8,128)(2,1)} async-done(((bf16[128,2048]{1,0:T(8,128)(2,1)}), bf16[64,2048]{1,0:T(8,128)(2,1)}) %reduce-scatter.2.cloned.1.call-update) | async-done | bytes 262160 | tf_op jit(solution)/shard_map/reduce_scatter | solution.py:73
  (8 shorter events, 0.1 us)
Async XLA Ops:
  6.5 73.0 %all-gather.2.cloned.1.call-start = ((), (), s32[]{:S(2)}) async-start(), calls=%async_computation.1 | async-start | bytes 2228224 | tf_op jit(solution)/shard_map/all_gather | solution.py:51
  9.0 4.8 %copy-start.1 = (f32[64]{0:T(128)S(1)}, f32[64]{0:T(128)}, u32[]{:S(2)}) copy-start(f32[64]{0:T(128)} %param.12) | copy-start | bytes 772
  9.0 4.9 %copy-start.2 = (f32[64]{0:T(128)S(1)}, f32[64]{0:T(128)}, u32[]{:S(2)}) copy-start(f32[64]{0:T(128)} %param.13) | copy-start | bytes 772
  13.8 97.0 %reduce-scatter.2.cloned.1.call-start = ((), (), s32[]{:S(2)}) async-start(), calls=%async_computation.2 | async-start | bytes 786432 | tf_op jit(solution)/shard_map/reduce_scatter | solution.py:73
  86.2 5.7 %copy-start = (f32[4,4,128,2048]{3,2,1,0:T(8,128)}, f32[4,4,128,2048]{3,2,1,0:T(8,128)S(1)}, u32[]{:S(2)}) copy-start(f32[4,4,128,2048]{3,2,1,0:T(8,128)S(1)} %get-tuple-element.20) | copy-start | bytes 50331652
Sparse Core Ops, SparseCore 0:
  13.9 65.5 all-gather.1
  104.6 6.0 reduce-scatter.1
where the time goes:
time: 118 us
  waiting for transfers between devices  70.1 us (59%)
  matrix products  19.1 us (16%)
  between operations  13.6 us (12%)
  other arithmetic  9.04 us (8%)
  local copies, waits for them, and re-layouts  3.27 us (3%)
  blocking collectives  2.5 us (2%)
    all_gather x1, waiting for transfers between devices, body(): piece = lax.all_gather(outgoing, 'sp', axis=0, tiled=True)  63.8 us
    dot_general x1, matrix products, body(): jnp.einsum('kgqn,nkd->kgqd', expo.astype(jnp.bfloat16), piece[:, key_cols...  8.83 us
    reduce_scatter x1, waiting for transfers between devices, body(): lax.psum_scatter(jnp.dot(mixed, w_out, preferred_element_type=jnp.float32...  6.26 us
    dot_general x1, matrix products, body(): jnp.dot(lax.all_gather(tokens_in, 'tp', axis=0, tiled=True), w_joined, pr...  4.06 us
    dot_general x1, matrix products, body(): jnp.dot(mixed, w_out, preferred_element_type=jnp.float32)  3.73 us
    reduce_sum x1, other arithmetic, body(): total = jnp.sum(expo, axis=-1)  3.27 us
    all_gather x1, blocking collectives, body(): lax.all_gather(tokens_in, 'tp', axis=0, tiled=True)  2.5 us
    dot_general x1, matrix products, body(): jnp.einsum('kgqd,nkd->kgqn', query_g, keys_n, preferred_element_type=jnp....  2.47 us
  transfers between devices with their start and end apart: 2, of which 2 were waited for; matrix products, arithmetic and copies ran while one was open for 1% of the time, Pallas kernels for 0%

commit v1 on v0

--- a/solution.py
+++ b/solution.py
@@ -48,7 +48,14 @@
     values = projected[:, query_cols + key_cols :]
     scale = head_dim ** (-0.5)
     outgoing = jnp.concatenate([raw_keys, values], axis=1)
-    piece = lax.all_gather(outgoing, "sp", axis=0, tiled=True)
+    size = lax.axis_size("sp")
+    route = [(i, (i + 1) % size) for i in range(size)]
+    parts = [outgoing]
+    for hop in range(1, size):
+        parts = [lax.ppermute(parts[0], "sp", route), *parts]
+    whole = jnp.concatenate(parts, axis=0)
+    turn = (lax.axis_index("sp") + 1) * parts[-1].shape[0]
+    piece = jnp.roll(whole, turn, axis=0)
     length = piece.shape[0]
     spot = jnp.arange(length, dtype=jnp.int32)
     keys_n = turned(

time: 118 us -> 180 us (1.53)
  waiting for transfers between devices: 70.1 us -> 132 us
  starting transfers between devices: 0.04 us -> 2.94 us
  other arithmetic: 9.04 us -> 6.26 us
    ppermute x0 -> x15, waiting for transfers between devices: none -> 128 us  [body(): parts = [lax.ppermute(parts[0], 'sp', route), *parts]]
    all_gather x1 -> x0, waiting for transfers between devices: 63.8 us -> none  [body(): piece = lax.all_gather(outgoing, 'sp', axis=0, tiled=True)]
    ppermute x0 -> x15, starting transfers between devices: none -> 2.94 us  [body(): parts = [lax.ppermute(parts[0], 'sp', route), *parts]]
    reduce_scatter x1, waiting for transfers between devices: 6.26 us -> 3.96 us  [body(): lax.psum_scatter(jnp.dot(mixed, w_out, preferred_element_type=jnp.float32...]
    unnamed x6 -> x37, local copies, waits for them, and re-layouts: 2.44 us -> 3.68 us
  transfers between devices with their start and end apart: 2 -> 16, of which waited for: 2 -> 16; matrix products, arithmetic and copies ran while one was open for 1% -> 1% of each run, Pallas kernels for 0% -> 0%
where the time goes in v1:
time: 180 us
  waiting for transfers between devices  132 us (73%)
  matrix products  19 us (11%)
  between operations  13.8 us (8%)
  other arithmetic  6.26 us (3%)
  local copies, waits for them, and re-layouts  3.9 us (2%)
  starting transfers between devices  2.94 us (2%)
  blocking collectives  2.5 us (1%)
    ppermute x15, waiting for transfers between devices, body(): parts = [lax.ppermute(parts[0], 'sp', route), *parts]  128 us
    dot_general x1, matrix products, body(): jnp.einsum('kgqn,nkd->kgqd', expo.astype(jnp.bfloat16), piece[:, key_cols...  8.8 us
    dot_general x1, matrix products, body(): jnp.dot(lax.all_gather(tokens_in, 'tp', axis=0, tiled=True), w_joined, pr...  4.02 us
    reduce_scatter x1, waiting for transfers between devices, body(): lax.psum_scatter(jnp.dot(mixed, w_out, preferred_element_type=jnp.float32...  3.96 us
    dot_general x1, matrix products, body(): jnp.dot(mixed, w_out, preferred_element_type=jnp.float32)  3.73 us
    unnamed x37, local copies, waits for them, and re-layouts  3.68 us
  transfers between devices with their start and end apart: 16, of which 16 were waited for; matrix products, arithmetic and copies ran while one was open for 1% of the time, Pallas kernels for 0%

profile of v1, /device:TPU:0, one launch (start us, length us, event | category | flops | bytes accessed | tf_op | source)
XLA Modules:
  0.0 180.3 jit_solution(16063612081057657763)
XLA Ops:
  6.5 2.5 %all_gather.3 = bf16[128,2048]{1,0:T(8,128)(2,1)S(1)} all-gather(bf16[64,2048]{1,0:T(8,128)(2,1)} %param.7), channel_id=1, replica_groups=mesh['sp'=16,'tp'=2] {'tp'}, dimensions={0}, use_global_device_ids=true | all-gather | bytes 786432 | tf_op jit(solution)/shard_map/all_gather | solution.py:33
  9.0 4.0 %fusion.13 = bf16[128,1536]{0,1:T(8,128)(2,1)S(1)} fusion(bf16[128,2048]{1,0:T(8,128)(2,1)S(1)} %all_gather.3, bf16[2048,256]{1,0:T(8,128)(2,1)} %param.10, bf16[2048,256]{1,0:T(8,128)(2,1)} %param.9, bf16[2048,1024]{1,0:T(8,128)(2,1)} %param.8), kind=kOutput, calls=%fused_computation.13 | convolution fusion | flops 824377344 | bytes 7208960 | tf_op jit(solution)/shard_map/dot_general | solution.py:32
  13.1 0.0 copy-start.2
  13.1 2.9 %collective-permute-start = (bf16[128,512]{0,1:T(8,128)(2,1)S(1)}, bf16[128,512]{0,1:T(8,128)(2,1)S(1)}, u32[]{:S(2)}, u32[]{:S(2)}) collective-permute-start(bf16[128,512]{0,1:T(8,128)(2,1)S(1)} %concatenate.31), channel_id=1, source_target_pairs={{0,2},{2,4},{4,6},{6,8},{8,10},{10,12},{12,14},{14,16},{16,18},{18... | collective-permute-start | bytes 393224 | tf_op jit(solution)/shard_map/ppermute | solution.py:55
  16.0 7.8 %collective-permute-done = bf16[128,512]{0,1:T(8,128)(2,1)S(1)} collective-permute-done((bf16[128,512]{0,1:T(8,128)(2,1)S(1)}, bf16[128,512]{0,1:T(8,128)(2,1)S(1)}, u32[]{:S(2)}, u32[]{:S(2)}) %collective-permute-start) | collective-permute-done | bytes 131104 | tf_op jit(solution)/shard_map/ppermute | solution.py:55
  23.8 0.0 collective-permute-start.1
  23.8 8.6 %collective-permute-done.1 = bf16[128,512]{0,1:T(8,128)(2,1)S(1)} collective-permute-done((bf16[128,512]{0,1:T(8,128)(2,1)S(1)}, bf16[128,512]{0,1:T(8,128)(2,1)S(1)}, u32[]{:S(2)}, u32[]{:S(2)}) %collective-permute-start.1) | collective-permute-done | bytes 131104 | tf_op jit(solution)/shard_map/ppermute | solution.py:55
  32.4 8.6 %collective-permute-done.2 = bf16[128,512]{0,1:T(8,128)(2,1)S(1)} collective-permute-done((bf16[128,512]{0,1:T(8,128)(2,1)S(1)}, bf16[128,512]{0,1:T(8,128)(2,1)S(1)}, u32[]{:S(2)}, u32[]{:S(2)}) %collective-permute-start.2) | collective-permute-done | bytes 131104 | tf_op jit(solution)/shard_map/ppermute | solution.py:55
  40.9 0.0 collective-permute-start.3
  40.9 8.6 %collective-permute-done.3 = bf16[128,512]{0,1:T(8,128)(2,1)S(1)} collective-permute-done((bf16[128,512]{0,1:T(8,128)(2,1)S(1)}, bf16[128,512]{0,1:T(8,128)(2,1)S(1)}, u32[]{:S(2)}, u32[]{:S(2)}) %collective-permute-start.3) | collective-permute-done | bytes 131104 | tf_op jit(solution)/shard_map/ppermute | solution.py:55
  49.5 8.6 %collective-permute-done.4 = bf16[128,512]{0,1:T(8,128)(2,1)S(1)} collective-permute-done((bf16[128,512]{0,1:T(8,128)(2,1)S(1)}, bf16[128,512]{0,1:T(8,128)(2,1)S(1)}, u32[]{:S(2)}, u32[]{:S(2)}) %collective-permute-start.4) | collective-permute-done | bytes 131104 | tf_op jit(solution)/shard_map/ppermute | solution.py:55
  58.0 0.0 collective-permute-start.5
  58.0 8.6 %collective-permute-done.5 = bf16[128,512]{0,1:T(8,128)(2,1)S(1)} collective-permute-done((bf16[128,512]{0,1:T(8,128)(2,1)S(1)}, bf16[128,512]{0,1:T(8,128)(2,1)S(1)}, u32[]{:S(2)}, u32[]{:S(2)}) %collective-permute-start.5) | collective-permute-done | bytes 131104 | tf_op jit(solution)/shard_map/ppermute | solution.py:55
  66.6 9.7 %collective-permute-done.6 = bf16[128,512]{0,1:T(8,128)(2,1)S(1)} collective-permute-done((bf16[128,512]{0,1:T(8,128)(2,1)S(1)}, bf16[128,512]{0,1:T(8,128)(2,1)S(1)}, u32[]{:S(2)}, u32[]{:S(2)}) %collective-permute-start.6) | collective-permute-done | bytes 131104 | tf_op jit(solution)/shard_map/ppermute | solution.py:55
  76.3 0.0 collective-permute-start.7
  76.3 0.1 broadcast_multiply_fusion.1
  76.4 0.1 mul.224
  76.5 8.9 %collective-permute-done.7 = bf16[128,512]{0,1:T(8,128)(2,1)S(1)} collective-permute-done((bf16[128,512]{0,1:T(8,128)(2,1)S(1)}, bf16[128,512]{0,1:T(8,128)(2,1)S(1)}, u32[]{:S(2)}, u32[]{:S(2)}) %collective-permute-start.7) | collective-permute-done | bytes 131104 | tf_op jit(solution)/shard_map/ppermute | solution.py:55
  85.4 0.0 collective-permute-start.8
  85.5 8.5 %collective-permute-done.8 = bf16[128,512]{0,1:T(8,128)(2,1)S(1)} collective-permute-done((bf16[128,512]{0,1:T(8,128)(2,1)S(1)}, bf16[128,512]{0,1:T(8,128)(2,1)S(1)}, u32[]{:S(2)}, u32[]{:S(2)}) %collective-permute-start.8) | collective-permute-done | bytes 131104 | tf_op jit(solution)/shard_map/ppermute | solution.py:55
  94.0 0.1 bitcast_reduce_fusion.1
  94.1 8.5 %collective-permute-done.9 = bf16[128,512]{0,1:T(8,128)(2,1)S(1)} collective-permute-done((bf16[128,512]{0,1:T(8,128)(2,1)S(1)}, bf16[128,512]{0,1:T(8,128)(2,1)S(1)}, u32[]{:S(2)}, u32[]{:S(2)}) %collective-permute-start.9) | collective-permute-done | bytes 131104 | tf_op jit(solution)/shard_map/ppermute | solution.py:55
  102.6 0.0 collective-permute-start.10
  102.6 8.6 %collective-permute-done.10 = bf16[128,512]{0,1:T(8,128)(2,1)S(1)} collective-permute-done((bf16[128,512]{0,1:T(8,128)(2,1)S(1)}, bf16[128,512]{0,1:T(8,128)(2,1)S(1)}, u32[]{:S(2)}, u32[]{:S(2)}) %collective-permute-start.10) | collective-permute-done | bytes 131104 | tf_op jit(solution)/shard_map/ppermute | solution.py:55
  111.1 0.1 multiply_multiply_fusion.1
  111.3 8.4 %collective-permute-done.11 = bf16[128,512]{0,1:T(8,128)(2,1)S(1)} collective-permute-done((bf16[128,512]{0,1:T(8,128)(2,1)S(1)}, bf16[128,512]{0,1:T(8,128)(2,1)S(1)}, u32[]{:S(2)}, u32[]{:S(2)}) %collective-permute-start.11) | collective-permute-done | bytes 131104 | tf_op jit(solution)/shard_map/ppermute | solution.py:55
  119.7 0.0 collective-permute-start.12
  119.7 0.1 broadcast_multiply_fusion.3
  119.8 0.1 fusion.34
  119.8 8.7 %collective-permute-done.12 = bf16[128,512]{0,1:T(8,128)(2,1)S(1)} collective-permute-done((bf16[128,512]{0,1:T(8,128)(2,1)S(1)}, bf16[128,512]{0,1:T(8,128)(2,1)S(1)}, u32[]{:S(2)}, u32[]{:S(2)}) %collective-permute-start.12) | collective-permute-done | bytes 131104 | tf_op jit(solution)/shard_map/ppermute | solution.py:55
  128.6 0.1 subtract_convert_fusion.1
  128.6 8.5 %collective-permute-done.13 = bf16[128,512]{0,1:T(8,128)(2,1)S(1)} collective-permute-done((bf16[128,512]{0,1:T(8,128)(2,1)S(1)}, bf16[128,512]{0,1:T(8,128)(2,1)S(1)}, u32[]{:S(2)}, u32[]{:S(2)}) %collective-permute-start.13) | collective-permute-done | bytes 131104 | tf_op jit(solution)/shard_map/ppermute | solution.py:55
  137.1 0.0 collective-permute-start.14
  137.1 0.9 fusion.27
  138.1 0.1 mul.244
  138.2 7.5 %collective-permute-done.14 = bf16[128,512]{0,1:T(8,128)(2,1)S(1)} collective-permute-done((bf16[128,512]{0,1:T(8,128)(2,1)S(1)}, bf16[128,512]{0,1:T(8,128)(2,1)S(1)}, u32[]{:S(2)}, u32[]{:S(2)}) %collective-permute-start.14) | collective-permute-done | bytes 131104 | tf_op jit(solution)/shard_map/ppermute | solution.py:55
  147.2 0.3 bitcast_reduce_fusion
  147.5 0.3 dynamic-slice_convert_fusion
  147.8 0.4 multiply_multiply_fusion
  148.3 0.3 subtract_convert_fusion
  148.6 0.1 pad_maximum_fusion
  148.7 2.5 %multiply_reduce_fusion = (f32[4,4,128]{2,1,0:T(4,128)S(1)}, f32[4,4,128,2048]{3,2,1,0:T(8,128)S(1)}) fusion(bf16[4,4,128,64]{2,3,1,0:T(8,128)(2,1)S(1)} %bitcast.38, bf16[2048,4,64,1]{0,2,3,1:T(8,128)(2,1)S(1)} %bitcast.36), kind=kOutput, calls=%fused_computation.1 | convolution fusion | flops 545257472 | bytes 18096128 | tf_op jit(solution)/shard_map/kgqd,nkd->kgqn/dot_general | solution.py:66
  151.2 3.3 %fusion = f32[4,4,128]{2,1,0:T(4,128)S(1)} fusion(f32[4,4,128,2048]{3,2,1,0:T(8,128)S(1)} %get-tuple-element.20, f32[4,4,128]{2,1,0:T(4,128)S(1)} %broadcast_maximum_fusion), kind=kLoop, calls=%fused_computation.2 | loop fusion | flops 12580864 | bytes 16793600 | tf_op jit(solution)/shard_map/reduce_sum | solution.py:70
  154.4 2.5 %copy-done = f32[4,4,128,2048]{3,2,1,0:T(8,128)} copy-done((f32[4,4,128,2048]{3,2,1,0:T(8,128)}, f32[4,4,128,2048]{3,2,1,0:T(8,128)S(1)}, u32[]{:S(2)}) %copy-start) | copy-done | bytes 16777240
  156.9 8.8 %fusion.22 = bf16[128,4,4,64]{0,3,2,1:T(8,128)(2,1)S(1)} fusion(bf16[2048,4,64,1]{0,2,3,1:T(8,128)(2,1)S(1)} %bitcast.39, f32[4,4,128,2048]{3,2,1,0:T(8,128)} %copy-done, f32[4,4,128]{2,1,0:T(4,128)S(1)} %broadcast_maximum_fusion, f32[128,4,4]{0,2,1:T(4,128)S(1)} %bitcast.41), kind=kOutput, calls=%fused_computation.22 | convolution fusion | flops 549715968 | bytes 18104320 | tf_op jit(solution)/shard_map/kgqn,nkd->kgqd/dot_general | solution.py:71
  165.7 3.7 %convolution_convert_fusion = bf16[128,2048]{1,0:T(8,128)(2,1)} fusion(bf16[128,1024]{0,1:T(8,128)(2,1)S(1)} %bitcast.40, bf16[1024,2048]{1,0:T(8,128)(2,1)} %param.11), kind=kOutput, calls=%fused_computation.12 | convolution fusion | flops 537133056 | bytes 4980736 | tf_op jit(solution)/shard_map/dot_general | solution.py:81
  169.4 0.0 reduce-scatter.2.cloned.1.call-update
  169.5 4.0 %reduce-scatter.2.cloned.1.call-done = bf16[64,2048]{1,0:T(8,128)(2,1)} async-done(((bf16[128,2048]{1,0:T(8,128)(2,1)}), bf16[64,2048]{1,0:T(8,128)(2,1)}) %reduce-scatter.2.cloned.1.call-update) | async-done | bytes 262160 | tf_op jit(solution)/shard_map/reduce_scatter | solution.py:80
  (52 shorter events, 1.4 us)
Async XLA Ops:
  6.5 166.9 %reduce-scatter.2.cloned.1.call-start = ((), (), s32[]{:S(2)}) async-start(), calls=%async_computation.1 | async-start | bytes 786432 | tf_op jit(solution)/shard_map/reduce_scatter | solution.py:80
  9.0 67.4 %copy-start.1 = (f32[64]{0:T(128)S(1)}, f32[64]{0:T(128)}, u32[]{:S(2)}) copy-start(f32[64]{0:T(128)} %param.12) | copy-start | bytes 772
  13.1 125.0 %copy-start.2 = (f32[64]{0:T(128)S(1)}, f32[64]{0:T(128)}, u32[]{:S(2)}) copy-start(f32[64]{0:T(128)} %param.13) | copy-start | bytes 772
  13.1 10.7 %collective-permute-start = (bf16[128,512]{0,1:T(8,128)(2,1)S(1)}, bf16[128,512]{0,1:T(8,128)(2,1)S(1)}, u32[]{:S(2)}, u32[]{:S(2)}) collective-permute-start(bf16[128,512]{0,1:T(8,128)(2,1)S(1)} %concatenate.31), channel_id=1, source_target_pairs={{0,2},{2,4},{4,6},{6,8},{8,10},{10,12},{12,14},{14,16},{16,18},{18... | collective-permute-start | bytes 393224 | tf_op jit(solution)/shard_map/ppermute | solution.py:55
  23.8 8.6 %collective-permute-start.1 = (bf16[128,512]{0,1:T(8,128)(2,1)S(1)}, bf16[128,512]{0,1:T(8,128)(2,1)S(1)}, u32[]{:S(2)}, u32[]{:S(2)}) collective-permute-start(bf16[128,512]{0,1:T(8,128)(2,1)S(1)} %collective-permute-done), channel_id=1, source_target_pairs={{0,2},{2,4},{4,6},{6,8},{8,10},{10,12},{12,14},{14,16},{16,18},{18... | collective-permute-start | bytes 393224 | tf_op jit(solution)/shard_map/ppermute | solution.py:55
  32.4 8.6 %collective-permute-start.2 = (bf16[128,512]{0,1:T(8,128)(2,1)S(1)}, bf16[128,512]{0,1:T(8,128)(2,1)S(1)}, u32[]{:S(2)}, u32[]{:S(2)}) collective-permute-start(bf16[128,512]{0,1:T(8,128)(2,1)S(1)} %collective-permute-done.1), channel_id=1, source_target_pairs={{0,2},{2,4},{4,6},{6,8},{8,10},{10,12},{12,14},{14,16},{16,18},{18... | collective-permute-start | bytes 393224 | tf_op jit(solution)/shard_map/ppermute | solution.py:55
  40.9 8.6 %collective-permute-start.3 = (bf16[128,512]{0,1:T(8,128)(2,1)S(1)}, bf16[128,512]{0,1:T(8,128)(2,1)S(1)}, u32[]{:S(2)}, u32[]{:S(2)}) collective-permute-start(bf16[128,512]{0,1:T(8,128)(2,1)S(1)} %collective-permute-done.2), channel_id=1, source_target_pairs={{0,2},{2,4},{4,6},{6,8},{8,10},{10,12},{12,14},{14,16},{16,18},{18... | collective-permute-start | bytes 393224 | tf_op jit(solution)/shard_map/ppermute | solution.py:55
  49.5 8.6 %collective-permute-start.4 = (bf16[128,512]{0,1:T(8,128)(2,1)S(1)}, bf16[128,512]{0,1:T(8,128)(2,1)S(1)}, u32[]{:S(2)}, u32[]{:S(2)}) collective-permute-start(bf16[128,512]{0,1:T(8,128)(2,1)S(1)} %collective-permute-done.3), channel_id=1, source_target_pairs={{0,2},{2,4},{4,6},{6,8},{8,10},{10,12},{12,14},{14,16},{16,18},{18... | collective-permute-start | bytes 393224 | tf_op jit(solution)/shard_map/ppermute | solution.py:55
  58.0 8.6 %collective-permute-start.5 = (bf16[128,512]{0,1:T(8,128)(2,1)S(1)}, bf16[128,512]{0,1:T(8,128)(2,1)S(1)}, u32[]{:S(2)}, u32[]{:S(2)}) collective-permute-start(bf16[128,512]{0,1:T(8,128)(2,1)S(1)} %collective-permute-done.4), channel_id=1, source_target_pairs={{0,2},{2,4},{4,6},{6,8},{8,10},{10,12},{12,14},{14,16},{16,18},{18... | collective-permute-start | bytes 393224 | tf_op jit(solution)/shard_map/ppermute | solution.py:55
  66.6 9.7 %collective-permute-start.6 = (bf16[128,512]{0,1:T(8,128)(2,1)S(1)}, bf16[128,512]{0,1:T(8,128)(2,1)S(1)}, u32[]{:S(2)}, u32[]{:S(2)}) collective-permute-start(bf16[128,512]{0,1:T(8,128)(2,1)S(1)} %collective-permute-done.5), channel_id=1, source_target_pairs={{0,2},{2,4},{4,6},{6,8},{8,10},{10,12},{12,14},{14,16},{16,18},{18... | collective-permute-start | bytes 393224 | tf_op jit(solution)/shard_map/ppermute | solution.py:55
  76.3 9.1 %collective-permute-start.7 = (bf16[128,512]{0,1:T(8,128)(2,1)S(1)}, bf16[128,512]{0,1:T(8,128)(2,1)S(1)}, u32[]{:S(2)}, u32[]{:S(2)}) collective-permute-start(bf16[128,512]{0,1:T(8,128)(2,1)S(1)} %collective-permute-done.6), channel_id=1, source_target_pairs={{0,2},{2,4},{4,6},{6,8},{8,10},{10,12},{12,14},{14,16},{16,18},{18... | collective-permute-start | bytes 393224 | tf_op jit(solution)/shard_map/ppermute | solution.py:55
  85.4 8.6 %collective-permute-start.8 = (bf16[128,512]{0,1:T(8,128)(2,1)S(1)}, bf16[128,512]{0,1:T(8,128)(2,1)S(1)}, u32[]{:S(2)}, u32[]{:S(2)}) collective-permute-start(bf16[128,512]{0,1:T(8,128)(2,1)S(1)} %collective-permute-done.7), channel_id=1, source_target_pairs={{0,2},{2,4},{4,6},{6,8},{8,10},{10,12},{12,14},{14,16},{16,18},{18... | collective-permute-start | bytes 393224 | tf_op jit(solution)/shard_map/ppermute | solution.py:55
  94.0 8.6 %collective-permute-start.9 = (bf16[128,512]{0,1:T(8,128)(2,1)S(1)}, bf16[128,512]{0,1:T(8,128)(2,1)S(1)}, u32[]{:S(2)}, u32[]{:S(2)}) collective-permute-start(bf16[128,512]{0,1:T(8,128)(2,1)S(1)} %collective-permute-done.8), channel_id=1, source_target_pairs={{0,2},{2,4},{4,6},{6,8},{8,10},{10,12},{12,14},{14,16},{16,18},{18... | collective-permute-start | bytes 393224 | tf_op jit(solution)/shard_map/ppermute | solution.py:55
  102.6 8.6 %collective-permute-start.10 = (bf16[128,512]{0,1:T(8,128)(2,1)S(1)}, bf16[128,512]{0,1:T(8,128)(2,1)S(1)}, u32[]{:S(2)}, u32[]{:S(2)}) collective-permute-start(bf16[128,512]{0,1:T(8,128)(2,1)S(1)} %collective-permute-done.9), channel_id=1, source_target_pairs={{0,2},{2,4},{4,6},{6,8},{8,10},{10,12},{12,14},{14,16},{16,18},{18... | collective-permute-start | bytes 393224 | tf_op jit(solution)/shard_map/ppermute | solution.py:55
  111.1 8.6 %collective-permute-start.11 = (bf16[128,512]{0,1:T(8,128)(2,1)S(1)}, bf16[128,512]{0,1:T(8,128)(2,1)S(1)}, u32[]{:S(2)}, u32[]{:S(2)}) collective-permute-start(bf16[128,512]{0,1:T(8,128)(2,1)S(1)} %collective-permute-done.10), channel_id=1, source_target_pairs={{0,2},{2,4},{4,6},{6,8},{8,10},{10,12},{12,14},{14,16},{16,18},{18... | collective-permute-start | bytes 393224 | tf_op jit(solution)/shard_map/ppermute | solution.py:55
  119.7 8.9 %collective-permute-start.12 = (bf16[128,512]{0,1:T(8,128)(2,1)S(1)}, bf16[128,512]{0,1:T(8,128)(2,1)S(1)}, u32[]{:S(2)}, u32[]{:S(2)}) collective-permute-start(bf16[128,512]{0,1:T(8,128)(2,1)S(1)} %collective-permute-done.11), channel_id=1, source_target_pairs={{0,2},{2,4},{4,6},{6,8},{8,10},{10,12},{12,14},{14,16},{16,18},{18... | collective-permute-start | bytes 393224 | tf_op jit(solution)/shard_map/ppermute | solution.py:55
  128.5 8.6 %collective-permute-start.13 = (bf16[128,512]{0,1:T(8,128)(2,1)S(1)}, bf16[128,512]{0,1:T(8,128)(2,1)S(1)}, u32[]{:S(2)}, u32[]{:S(2)}) collective-permute-start(bf16[128,512]{0,1:T(8,128)(2,1)S(1)} %collective-permute-done.12), channel_id=1, source_target_pairs={{0,2},{2,4},{4,6},{6,8},{8,10},{10,12},{12,14},{14,16},{16,18},{18... | collective-permute-start | bytes 393224 | tf_op jit(solution)/shard_map/ppermute | solution.py:55
  137.1 8.6 %collective-permute-start.14 = (bf16[128,512]{0,1:T(8,128)(2,1)S(1)}, bf16[128,512]{0,1:T(8,128)(2,1)S(1)}, u32[]{:S(2)}, u32[]{:S(2)}) collective-permute-start(bf16[128,512]{0,1:T(8,128)(2,1)S(1)} %collective-permute-done.13), channel_id=1, source_target_pairs={{0,2},{2,4},{4,6},{6,8},{8,10},{10,12},{12,14},{14,16},{16,18},{18... | collective-permute-start | bytes 393224 | tf_op jit(solution)/shard_map/ppermute | solution.py:55
  151.1 5.7 %copy-start = (f32[4,4,128,2048]{3,2,1,0:T(8,128)}, f32[4,4,128,2048]{3,2,1,0:T(8,128)S(1)}, u32[]{:S(2)}) copy-start(f32[4,4,128,2048]{3,2,1,0:T(8,128)S(1)} %get-tuple-element.20) | copy-start | bytes 50331652
Sparse Core Ops, SparseCore 0:
  169.6 3.7 reduce-scatter.1
